TPU v7x, 32 devices: a whole 2x2x4 slice. The times are simulated.
32 devices in a mesh: sp: 8 (over z, core), tp: 4 (over y, x).
Axes of the slice: x: 2, y: 2, z: 4, core: 2. Of those that a mesh axis runs over, the one named last changes fastest.
Arguments:
- outer_gate: bfloat16 [2048, 1024], P('sp', 'tp'), may hold values from -6 to 6
- inner_gate: bfloat16 [2048, 1024], P('sp', 'tp'), may hold values from -6 to 6
- values: bfloat16 [2048, 1024], P('sp', 'tp'), may hold values from -6 to 6
- conv_taps: bfloat16 [3, 1024], P(None, 'tp'), may hold values from -3.5 to 3.5
- document: int32 [2048], P('sp'), may hold values from 0 to 3, never falling along the last dimension, each value on 1 to 1024 neighbouring positions
- mix_proj: bfloat16 [1024, 2048], P('tp'), may hold values from -0.1875 to 0.1875
- stream: bfloat16 [2048, 2048], P('sp'), may hold values from -6 to 6
- norm_gain: float32 [2048], replicated, may hold values from 0.1 to 1.9
- routes: int32 [2048, 2], P('sp'), may hold values from 0 to 7, all different within a row; in each aligned block of 256 rows (0 to 255, 256 to 511, ...) at most 96 rows name the same one
- route_weight: float32 [2048, 2], P('sp'), may hold values from 0.25 to 1
- w_gate: bfloat16 [8, 2048, 4096], P('sp', None, 'tp'), may hold values from -0.125 to 0.125
- w_up: bfloat16 [8, 2048, 4096], P('sp', None, 'tp'), may hold values from -0.125 to 0.125
- w_down: bfloat16 [8, 4096, 2048], P('sp', 'tp'), may hold values from -0.09375 to 0.09375
Outputs:
- mixed: bfloat16 [2048, 2048], P('sp', 'tp')
Inputs may be any that keep to these rules, and one draw needn't show every extreme that they name: Document numbers never fall along the sequence; each document holds 1 to 1024 consecutive tokens and one holds exactly that many. `routes`: each token names 2 different experts. Among the 256 tokens of one sp index no expert is named by more than 96 tokens, and in some sp index's tokens an expert is named by exactly 96.
All inputs are finite; a program needn't handle non-finite values.
Results may differ from a plain program's by a relative error of at most 0.014.
Values may be sent and summed in bfloat16 or wider, within the bound.
A program may use at most 64 MiB of HBM per device.

v0:
```python
import functools

import jax
import jax.numpy as jnp
from jax import lax
from jax.experimental import pallas as pl
from jax.experimental.pallas import tpu as pltpu
from jax.sharding import PartitionSpec as P

F32 = jnp.float32
BF16 = jnp.bfloat16
MESH = pl.DeviceIdType.MESH
GROUP = 1
HEAD = 16


def xor(value, mask, count):
    out, bit = value, 1
    while bit < count:
        if isinstance(mask, int):
            if mask & bit:
                out = out + bit * (1 - 2 * lax.rem(lax.div(value, bit), 2))
        else:
            ours = lax.rem(lax.div(value, bit), 2)
            other = lax.rem(lax.div(mask, bit), 2)
            out = out + bit * other * (1 - 2 * ours)
        bit *= 2
    return out


def kernel(
    n_sp, n_tp, cap,
    taps, doc_r, routes_r, rw_r, gain,
    outer_hbm, inner_hbm, vals_hbm, mix_hbm, stream_hbm, wg_hbm, wu_hbm, wd_hbm,
    out,
    outer, inner, vals, mix, own, wg, wu, wd, rim_out, rim_in, prod_pad, doc_pad,
    bpart, brecv, head, hidden, obuf, xbuf, pbuf, r1, act, ret, back, acc,
    local_sem, rim_s, rim_r, br_s, br_r, hd_s, hd_r, z_s, z_r, ag_s, ag_r, rs_s, rs_r, bk_s, bk_r,
):
    s, p = lax.axis_index("sp"), lax.axis_index("tp")
    length, channels = outer.shape
    width = own.shape[1]
    features = mix.shape[1]
    hidden_units = wg.shape[1]
    x_side = 1
    while x_side * x_side < n_tp:
        x_side *= 2
    x_set = list(range(x_side))
    y_set = [k * x_side for k in range(n_tp // x_side)]

    def at(index):
        return pl.multiple_of(index * width, width)

    loads = [
        pltpu.make_async_copy(inner_hbm, inner, local_sem.at[0]),
        pltpu.make_async_copy(vals_hbm, vals, local_sem.at[1]),
        pltpu.make_async_copy(outer_hbm, outer, local_sem.at[2]),
        pltpu.make_async_copy(mix_hbm, mix, local_sem.at[3]),
        pltpu.make_async_copy(stream_hbm.at[:, pl.ds(at(p), width)], own, local_sem.at[4]),
    ]
    weight_loads = [
        pltpu.make_async_copy(wg_hbm.at[0], wg, local_sem.at[5]),
        pltpu.make_async_copy(wu_hbm.at[0], wu, local_sem.at[6]),
        pltpu.make_async_copy(wd_hbm.at[0], wd, local_sem.at[7]),
    ]
    for load in loads:
        load.start()

    barrier = pltpu.get_barrier_semaphore()
    for d in range(1, n_sp):
        pl.semaphore_signal(barrier, inc=1, device_id={"sp": xor(s, d, n_sp)}, device_id_type=MESH)
    for r in range(1, n_tp):
        pl.semaphore_signal(barrier, inc=1, device_id={"tp": xor(p, r, n_tp)}, device_id_type=MESH)
    lines = [routes_r[...].astype(F32), rw_r[...], doc_r[...].astype(F32)]
    table = jnp.concatenate(lines + [jnp.zeros((3, length), F32)], axis=0)
    table = jnp.concatenate([table] * 16, axis=0).T
    chosen = [table[:, 0:1], table[:, 1:2]]
    chosen_weight = [table[:, 2:3], table[:, 3:4]]
    docs = jnp.broadcast_to(table[:, 4:5], (length, channels))
    loads[0].wait()
    loads[1].wait()
    product = inner[...].astype(F32) * vals[...].astype(F32)
    prod_pad[8:, :] = product
    doc_pad[8:, :] = docs
    rim_out[:8, :] = product[length - 8 :]
    rim_out[8:, :] = docs[length - 8 :]
    kernel_taps = taps[...].astype(F32)

    def gated(count):
        conv = kernel_taps[2:3] * product[:count]
        for step in (1, 2):
            same = doc_pad[pl.ds(8 - step, count), :] == docs[:count]
            before = prod_pad[pl.ds(8 - step, count), :]
            conv = conv + kernel_taps[2 - step : 3 - step] * jnp.where(same, before, 0.0)
        return (outer[:count, :].astype(F32) * conv).astype(BF16)

    def branch_part(rows, r):
        lanes = pl.ds(at(xor(p, r, n_tp)), width)
        return jnp.dot(rows, mix[:, lanes], preferred_element_type=F32).astype(BF16)

    prod_pad[:8, :] = jnp.zeros((8, channels), F32)
    doc_pad[:8, :] = jnp.full((8, channels), -1.0, F32)
    loads[2].wait()
    loads[3].wait()
    rows = gated(length)
    for r in range(n_tp):
        bpart[r] = branch_part(rows, r)
    pl.semaphore_wait(barrier, n_sp - 1 + n_tp - 1)

    sends = []

    def send(src, dst, s_sem, r_sem, **device):
        copy = pltpu.make_async_remote_copy(
            src_ref=src, dst_ref=dst, send_sem=s_sem, recv_sem=r_sem,
            device_id=device, device_id_type=MESH,
        )
        copy.start()
        sends.append(copy)
        return copy

    rim = send(rim_out, rim_in, rim_s, rim_r, sp=lax.rem(s + 1, n_sp))
    for r in range(n_tp - 1, 0, -1):
        rest = pl.ds(HEAD, length - HEAD)
        send(bpart.at[r, rest], brecv.at[r, rest], br_s.at[r], br_r.at[r], tp=xor(p, r, n_tp))
    for load in weight_loads:
        load.start()

    row = lax.broadcasted_iota(jnp.int32, (length, length), 0)
    col = lax.broadcasted_iota(jnp.int32, (length, length), 1)
    expert_r = lax.broadcasted_iota(jnp.int32, (max(n_sp, 16), length), 0)
    in_r = ((routes_r[0:1, :] == expert_r) | (routes_r[1:2, :] == expert_r)).astype(F32)
    rank_r = jnp.dot(in_r.astype(BF16), (row < col).astype(F32).astype(BF16), preferred_element_type=F32)
    expert_c = lax.broadcasted_iota(jnp.int32, (length, 128), 1).astype(F32)
    in_c = ((chosen[0] == expert_c) | (chosen[1] == expert_c)).astype(F32)
    rank_c = jnp.dot((row > col).astype(F32).astype(BF16), in_c.astype(BF16), preferred_element_type=F32)
    rank_r = jnp.where(in_r > 0, rank_r, -1.0)
    rank_c = jnp.where(in_c > 0, rank_c, -1.0)

    rim.wait_recv()
    prod_pad[:8, :] = rim_in[:8, :]
    doc_pad[:8, :] = jnp.where(s > 0, rim_in[8:, :], -1.0)
    rows = gated(HEAD)
    for r in range(n_tp - 1, -1, -1):
        head[r] = branch_part(rows, r)
        if r:
            send(head.at[r], brecv.at[r, pl.ds(0, HEAD)], hd_s.at[r], hd_r.at[r], tp=xor(p, r, n_tp))
    bpart[0, :HEAD] = head[0]
    loads[4].wait()
    total = bpart[0].astype(F32)
    for r in range(1, n_tp):
        for rows, sem in ((pl.ds(HEAD, length - HEAD), br_r), (pl.ds(0, HEAD), hd_r)):
            pltpu.make_async_copy(brecv.at[r, rows], brecv.at[r, rows], sem.at[r]).wait()
        total = total + brecv[r].astype(F32)
    total = total + own[...].astype(F32)
    hidden[...] = total
    scaled = (total * gain[:, pl.ds(at(p), width)]).astype(BF16)

    slot_r = lax.broadcasted_iota(jnp.int32, (cap, length), 0).astype(F32)
    turn = [0, 2, 4, 6, 3, 5, 7, 1] + list(range(8, n_sp))
    for d in range(n_sp):
        e = xor(s, turn[d], n_sp)
        line = jnp.sum(jnp.where(expert_r == e, rank_r, 0.0), axis=0, keepdims=True)
        pick = (line == slot_r).astype(F32).astype(BF16)
        rows = jnp.dot(pick, scaled, preferred_element_type=F32).astype(BF16)
        if d == 0:
            xbuf[0, 0] = rows
        else:
            obuf[d] = rows
            send(obuf.at[d], xbuf.at[0, d], z_s.at[d], z_r.at[d], sp=e)

    def arrived(ref, sem):
        pltpu.make_async_copy(ref, ref, sem).wait()

    def axes(d):
        return (x_set, y_set) if d % 2 == 0 else (y_set, x_set)

    def gather_first(d):
        first, _ = axes(d)
        if d:
            arrived(xbuf.at[0, d], z_r.at[d])
        for f in first[1:]:
            send(xbuf.at[0, d], xbuf.at[f, d], ag_s.at[d, f], ag_r.at[d, f], tp=xor(p, f, n_tp))

    def gather_second(d):
        first, second = axes(d)
        for f in first:
            if f:
                arrived(xbuf.at[f, d], ag_r.at[d, f])
            for g in second[1:]:
                send(
                    xbuf.at[f, d], xbuf.at[f + g, d], ag_s.at[d, f + g], ag_r.at[d, f + g],
                    tp=xor(p, g, n_tp),
                )

    tile = min(256, hidden_units)

    def expert_up(low):
        for d in range(low, low + GROUP):
            first, second = axes(d)
            for f in first:
                for g in second[1:]:
                    arrived(xbuf.at[f + g, d], ag_r.at[d, f + g])
        square = jnp.zeros((GROUP * cap, 1), F32)
        for r in range(n_tp):
            inverse = 1.0 / gain[:, pl.ds(at(xor(p, r, n_tp)), width)]
            plain = xbuf[r, low : low + GROUP].reshape(GROUP * cap, width).astype(F32) * inverse
            square = square + jnp.sum(plain * plain, axis=1, keepdims=True)
        scale = lax.rsqrt(square / features + 1e-06)

        def up_tile(j, _):
            lanes = pl.ds(pl.multiple_of(j * tile, tile), tile)
            gate = jnp.zeros((GROUP * cap, tile), F32)
            upper = jnp.zeros((GROUP * cap, tile), F32)
            for r in range(n_tp):
                lhs = xbuf[r, low : low + GROUP].reshape(GROUP * cap, width)
                deep = pl.ds(at(xor(p, r, n_tp)), width)
                gate = gate + jnp.dot(lhs, wg[deep, lanes], preferred_element_type=F32)
                upper = upper + jnp.dot(lhs, wu[deep, lanes], preferred_element_type=F32)
            gate, upper = gate * scale, upper * scale
            act[:, lanes] = (gate / (1.0 + jnp.exp(-gate)) * upper).astype(BF16)
            return 0

        lax.fori_loop(0, hidden_units // tile, up_tile, 0)

    def expert_down(low):
        for r in range(n_tp - 1, -1, -1):
            lanes = pl.ds(at(xor(p, r, n_tp)), width)
            part = jnp.dot(act[...], wd[:, lanes], preferred_element_type=F32).astype(BF16)
            pbuf[r, low : low + GROUP] = part.reshape(GROUP, cap, width)
            for d in range(low, low + GROUP):
                first, second = axes(d)
                for f in first[1:]:
                    if r - f in second:
                        send(
                            pbuf.at[r, d], r1.at[r, d], rs_s.at[d, r], rs_r.at[d, r],
                            tp=xor(p, f, n_tp),
                        )

    def scatter_second(d):
        first, second = axes(d)
        for g in second[1:]:
            part = pbuf[g, d].astype(F32)
            for f in first[1:]:
                arrived(r1.at[f + g, d], rs_r.at[d, f + g])
                part = part + r1[f + g, d].astype(F32)
            pbuf[g, d] = part.astype(BF16)
            send(pbuf.at[g, d], r1.at[g, d], rs_s.at[d, g], rs_r.at[d, g], tp=xor(p, g, n_tp))

    def give_back(d):
        first, second = axes(d)
        part = pbuf[0, d].astype(F32)
        for k in first[1:] + second[1:]:
            arrived(r1.at[k, d], rs_r.at[d, k])
            part = part + r1[k, d].astype(F32)
        if d == 0:
            back[0] = part.astype(BF16)
        else:
            ret[d] = part.astype(BF16)
            send(ret.at[d], back.at[d], bk_s.at[d], bk_r.at[d], sp=xor(s, turn[d], n_sp))

    slot_c = lax.broadcasted_iota(jnp.int32, (length, cap), 1).astype(F32)
    acc[...] = hidden[...]

    def combine(d):
        e = xor(s, turn[d], n_sp)
        if d:
            arrived(back.at[d], bk_r.at[d])
        line = jnp.sum(jnp.where(expert_c == e.astype(F32), rank_c, 0.0), axis=1, keepdims=True)
        pick = (line == slot_c).astype(F32).astype(BF16)
        fetched = jnp.dot(pick, back[d], preferred_element_type=F32)
        weight = sum(jnp.where(c == e.astype(F32), w, 0.0) for c, w in zip(chosen, chosen_weight))
        acc[...] = acc[...] + fetched * weight

    def run(stage, *steps):
        for step in steps:
            if 0 <= step < count:
                low = step * GROUP
                if stage in (expert_up, expert_down):
                    stage(low)
                else:
                    for d in range(low, low + GROUP):
                        stage(d)

    count = n_sp // GROUP
    run(gather_first, 0)
    run(gather_first, 1)
    run(gather_second, 0)
    run(gather_first, 2)
    run(gather_second, 1)
    run(gather_first, 3)
    run(gather_second, 2)
    for load in weight_loads:
        load.wait()
    for step in range(count + 8):
        run(expert_up, step + 0)
        run(gather_first, step + 4)
        run(gather_second, step + 3)
        run(expert_down, step + 0)
        run(scatter_second, step - 2)
        run(give_back, step - 4)
        run(combine, step - 6)
    out[...] = acc[...].astype(out.dtype)
    for copy in sends:
        copy.wait_send()


def body(
    outer_gate, inner_gate, values, conv_taps, document, mix_proj, stream, norm_gain,
    routes, route_weight, w_gate, w_up, w_down,
):
    length, features = stream.shape
    channels = outer_gate.shape[1]
    n_sp, n_tp = lax.axis_size("sp"), lax.axis_size("tp")
    width = features // n_tp
    units = w_gate.shape[2]
    cap = -(-(3 * length // n_sp) // 16) * 16
    vmem, anywhere = pl.BlockSpec(memory_space=pltpu.VMEM), pl.BlockSpec(memory_space=pl.ANY)
    block = (n_sp, cap, width)
    dma = pltpu.SemaphoreType.DMA
    return pl.pallas_call(
        functools.partial(kernel, n_sp, n_tp, cap),
        out_shape=jax.ShapeDtypeStruct((length, width), BF16),
        in_specs=[vmem] * 5 + [anywhere] * 8,
        out_specs=vmem,
        scratch_shapes=[
            pltpu.VMEM((length, channels), BF16),
            pltpu.VMEM((length, channels), BF16),
            pltpu.VMEM((length, channels), BF16),
            pltpu.VMEM((channels, features), BF16),
            pltpu.VMEM((length, width), BF16),
            pltpu.VMEM((features, units), BF16),
            pltpu.VMEM((features, units), BF16),
            pltpu.VMEM((units, features), BF16),
            pltpu.VMEM((16, channels), F32),
            pltpu.VMEM((16, channels), F32),
            pltpu.VMEM((length + 8, channels), F32),
            pltpu.VMEM((length + 8, channels), F32),
            pltpu.VMEM((n_tp, length, width), BF16),
            pltpu.VMEM((n_tp, length, width), BF16),
            pltpu.VMEM((n_tp, HEAD, width), BF16),
            pltpu.VMEM((length, width), F32),
            pltpu.VMEM(block, BF16),
            pltpu.VMEM((n_tp,) + block, BF16),
            pltpu.VMEM((n_tp,) + block, BF16),
            pltpu.VMEM((n_tp,) + block, BF16),
            pltpu.VMEM((GROUP * cap, units), BF16),
            pltpu.VMEM(block, BF16),
            pltpu.VMEM(block, BF16),
            pltpu.VMEM((length, width), F32),
            dma((8,)), dma, dma, dma((n_tp,)), dma((n_tp,)), dma((n_tp,)), dma((n_tp,)), dma((n_sp,)), dma((n_sp,)),
            dma((n_sp, n_tp)), dma((n_sp, n_tp)), dma((n_sp, n_tp)), dma((n_sp, n_tp)),
            dma((n_sp,)), dma((n_sp,)),
        ],
        compiler_params=pltpu.CompilerParams(
            collective_id=0, has_side_effects=True, vmem_limit_bytes=56 << 20
        ),
    )(
        conv_taps, document.reshape(1, -1), routes.T, route_weight.T, norm_gain.reshape(1, -1),
        outer_gate, inner_gate, values, mix_proj, stream, w_gate, w_up, w_down,
    )


def solution(mesh):
    return jax.shard_map(
        body,
        mesh=mesh,
        in_specs=(
            P("sp", "tp"),
            P("sp", "tp"),
            P("sp", "tp"),
            P(None, "tp"),
            P("sp"),
            P("tp", None),
            P("sp", None),
            P(),
            P("sp", None),
            P("sp", None),
            P("sp", None, "tp"),
            P("sp", None, "tp"),
            P("sp", "tp", None),
        ),
        out_specs=P("sp", "tp"),
        check_vma=False,
    )
```

profile of v0, /device:TPU:1, one launch (start us, length us, event | category | flops | bytes accessed | tf_op | source)
XLA Modules:
  0.0 88.4 jit_solution(3132293388823893181)
XLA Ops:
  0.0 86.7 %shard_map.127 = bf16[256,512]{1,0:T(8,128)(2,1)} custom-call(bf16[3,256]{1,0:T(4,128)(2,1)} %taps.1, s32[1,256]{1,0:T(1,128)} %bitcast.7, s32[2,256]{1,0:T(2,128)} %bitcast.5, f32[2,256]{1,0:T(2,128)} %bitcast.6, f32[1,2048]{1,0:T(1,128)} %bitcast.4, bf16[256,256]{1,0:T(8,128)(2,1)} %outer_hbm.1, bf16[256,256]{1,0:T(8,128)(2,1)} %inner_hbm.1, ...), custom_call_target="tpu_custom_call" | custom-call | tf_op jit(solution)/shard_map/pallas_call | solution.py:320
  86.7 1.7 %copy.15 = bf16[256,512]{1,0:T(8,128)(2,1)} copy(bf16[256,512]{1,0:T(8,128)(2,1)} %shard_map.127) | data formatting | bytes 524288
where the time goes:
time: 88.6 us; the launch traced here: 88.4 us
  Pallas kernels  86.7 us (98%)
  local copies, waits for them, and re-layouts  1.67 us (2%)
    pallas_call x1, Pallas kernels, body(): pl.pallas_call(functools.partial(kernel, n_sp, n_tp, cap), out_shape=jax....  86.7 us

commit v1 on v0

v1 whole, which is shorter than its diff:
```python
import functools

import jax
import jax.numpy as jnp
from jax import lax
from jax.experimental import pallas as pl
from jax.experimental.pallas import tpu as pltpu
from jax.sharding import PartitionSpec as P

F32 = jnp.float32
BF16 = jnp.bfloat16
MESH = pl.DeviceIdType.MESH
HEAD = 16
TUNED = (
    (0, 1), (0, 0), (1, 0), (1, 1), (0, 2), (0, 3), (0, 4), (1, 2), (2, 1), (1, 3),
    (0, 5), (1, 4), (3, 1), (4, 1), (6, 1), (0, 6), (1, 5), (2, 2), (0, 7), (3, 2),
    (4, 2), (6, 2), (1, 6), (2, 3), (5, 2), (3, 3), (4, 3), (5, 3), (1, 7), (6, 3),
    (2, 4), (3, 4), (4, 4), (6, 4), (2, 6), (7, 2), (5, 4), (3, 6), (7, 3), (4, 6),
    (6, 6), (5, 6), (2, 5), (8, 2), (3, 5), (4, 5), (7, 4), (5, 5), (6, 5), (8, 3),
    (2, 7), (3, 7), (7, 6), (4, 7), (8, 4), (5, 7), (6, 7), (2, 0), (9, 3), (7, 5),
    (8, 6), (9, 2), (5, 1), (3, 0), (4, 0), (6, 0), (7, 7), (8, 5), (5, 0), (8, 7),
    (7, 1), (9, 4), (7, 0), (9, 6), (9, 5), (8, 1), (9, 1), (9, 7), (8, 0), (9, 0),
)


def general_plan(n_sp):
    plan, near = [], min(2, n_sp)

    def run(k, d, low=0):
        if low <= d < n_sp and (k, d) not in plan:
            plan.append((k, d))

    for k, d in ((0, 0), (0, 1), (1, 0), (0, 2), (1, 1), (0, 3)):
        run(k, d)
    for d in range(n_sp):
        run(2, d)
        run(1, d + 2)
        run(3, d)
        run(0, d + 4)
        run(4, d)
        run(5, d, near)
        run(6, d)
        run(7, d - 2, near)
        run(8, d - 4, near)
        run(9, d - 7, near)
    for d in (n_sp - 2, n_sp - 1):
        run(8, d - 2, near)
        run(7, d, near)
        run(5, n_sp - 1 - d)
    for d in range(near, n_sp):
        run(8, d)
    for d in (1, 0):
        run(7, d)
    for d in range(near, n_sp - 2):
        run(9, d)
    for d in (1, 0):
        run(8, d)
    for d in range(n_sp):
        run(9, d)
    return plan


def xor(value, mask, count):
    out, bit = value, 1
    while bit < count:
        if isinstance(mask, int):
            if mask & bit:
                out = out + bit * (1 - 2 * lax.rem(lax.div(value, bit), 2))
        else:
            ours = lax.rem(lax.div(value, bit), 2)
            other = lax.rem(lax.div(mask, bit), 2)
            out = out + bit * other * (1 - 2 * ours)
        bit *= 2
    return out


def kernel(
    n_sp, n_tp, cap,
    taps_hbm, doc_hbm, routes_hbm, rw_hbm, gain_hbm, outer_hbm, inner_hbm, vals_hbm, mix_hbm, stream_hbm, wg_hbm, wu_hbm, wd_hbm,
    out,
    taps, doc_r, routes_r, rw_r, gain, outer, inner, vals, own, wg, wu, wd, rim_out, rim_in, prod_pad, doc_pad,
    gbuf, mixb, hidden, obuf, xbuf, pbuf, r1, act, ret, back, acc,
    local_sem, rim_s, rim_r, ga_s, ga_r, mx_s, mx_r, z_s, z_r, ag_s, ag_r, rs_s, rs_r, bk_s, bk_r,
):
    s, p = lax.axis_index("sp"), lax.axis_index("tp")
    length, channels = outer.shape
    width = own.shape[1]
    features = mix_hbm.shape[1]
    hidden_units = wg.shape[1]
    x_side = 1
    while x_side * x_side < n_tp:
        x_side *= 2
    square = x_side * x_side == n_tp
    firsts, seconds = range(x_side), range(n_tp // x_side)

    def at(index):
        return pl.multiple_of(index * width, width)

    loads = [
        pltpu.make_async_copy(inner_hbm, inner, local_sem.at[0]),
        pltpu.make_async_copy(vals_hbm, vals, local_sem.at[1]),
        pltpu.make_async_copy(outer_hbm, outer, local_sem.at[2]),
        pltpu.make_async_copy(mix_hbm.at[:, pl.ds(at(p), width)], mixb.at[0], local_sem.at[3]),
        pltpu.make_async_copy(stream_hbm.at[:, pl.ds(at(p), width)], own, local_sem.at[4]),
    ]
    weight_loads = [
        pltpu.make_async_copy(wg_hbm.at[0], wg, local_sem.at[5]),
        pltpu.make_async_copy(wu_hbm.at[0], wu, local_sem.at[6]),
        pltpu.make_async_copy(wd_hbm.at[0], wd, local_sem.at[7]),
    ]
    small_loads = [
        pltpu.make_async_copy(src, dst, local_sem.at[8 + k])
        for k, (src, dst) in enumerate(
            ((routes_hbm, routes_r), (rw_hbm, rw_r), (doc_hbm, doc_r), (taps_hbm, taps), (gain_hbm, gain))
        )
    ]
    for load in small_loads + loads:
        load.start()

    barrier = pltpu.get_barrier_semaphore()
    for d in range(1, n_sp):
        pl.semaphore_signal(barrier, inc=1, device_id={"sp": xor(s, d, n_sp)}, device_id_type=MESH)
    for r in range(1, n_tp):
        pl.semaphore_signal(barrier, inc=1, device_id={"tp": xor(p, r, n_tp)}, device_id_type=MESH)
    sends = []

    def send(src, dst, s_sem, r_sem, **device):
        copy = pltpu.make_async_remote_copy(
            src_ref=src, dst_ref=dst, send_sem=s_sem, recv_sem=r_sem,
            device_id=device, device_id_type=MESH,
        )
        copy.start()
        sends.append(copy)
        return copy

    def arrived(ref, sem):
        pltpu.make_async_copy(ref, ref, sem).wait()

    masks = [m for m in (2, 1) if m < n_sp]
    pieces = 2 ** len(masks)
    piece = channels // pieces

    def piece_rows(mask):
        return pl.ds(pl.multiple_of(lax.rem(xor(s, mask, n_sp), pieces) * piece, piece), piece)

    pl.semaphore_wait(barrier, n_sp - 1 + n_tp - 1)
    for r in range(n_tp - 1, 0, -1):
        peer = xor(p, r, n_tp)
        send(
            mix_hbm.at[piece_rows(0), pl.ds(at(peer), width)], mixb.at[r, piece_rows(0)],
            mx_s.at[0, r], mx_r.at[0, r], tp=peer,
        )

    def pass_on(r, mask, step):
        send(
            mixb.at[r, piece_rows(mask)], mixb.at[r, piece_rows(mask)],
            mx_s.at[step, r], mx_r.at[step, r], sp=xor(s, masks[-1] if step != 1 else masks[0], n_sp),
        )

    for load in small_loads:
        load.wait()
    lines = [routes_r[...].astype(F32), rw_r[...], doc_r[...].astype(F32)]
    table = jnp.concatenate(lines + [jnp.zeros((3, length), F32)], axis=0)
    table = jnp.concatenate([table] * 16, axis=0).T
    chosen = [table[:, 0:1], table[:, 1:2]]
    chosen_weight = [table[:, 2:3], table[:, 3:4]]
    docs = jnp.broadcast_to(table[:, 4:5], (length, channels))
    loads[0].wait()
    loads[1].wait()
    product = inner[...].astype(F32) * vals[...].astype(F32)
    prod_pad[8:, :] = product
    doc_pad[8:, :] = docs
    rim_out[:8, :] = product[length - 8 :]
    rim_out[8:, :] = docs[length - 8 :]
    kernel_taps = taps[...].astype(F32)

    def gated(count):
        conv = kernel_taps[2:3] * product[:count]
        for step in (1, 2):
            same = doc_pad[pl.ds(8 - step, count), :] == docs[:count]
            before = prod_pad[pl.ds(8 - step, count), :]
            conv = conv + kernel_taps[2 - step : 3 - step] * jnp.where(same, before, 0.0)
        return (outer[:count, :].astype(F32) * conv).astype(BF16)

    has_next = s < n_sp - 1
    rim = pltpu.make_async_remote_copy(
        src_ref=rim_out, dst_ref=rim_in, send_sem=rim_s, recv_sem=rim_r,
        device_id={"sp": lax.rem(s + 1, n_sp)}, device_id_type=MESH,
    )

    @pl.when(has_next)
    def _():
        rim.start()

    prod_pad[:8, :] = jnp.zeros((8, channels), F32)
    doc_pad[:8, :] = jnp.full((8, channels), -1.0, F32)
    loads[2].wait()
    gbuf[0] = gated(length)

    @pl.when(s > 0)
    def _():
        rim.wait_recv()
        prod_pad[:8, :] = rim_in[:8, :]
        doc_pad[:8, :] = rim_in[8:, :]
        gbuf[0, :HEAD] = gated(HEAD)

    for r in range(n_tp - 1, 0, -1):
        send(gbuf.at[0], gbuf.at[r], ga_s.at[r], ga_r.at[r], tp=xor(p, r, n_tp))
    for load in weight_loads:
        load.start()

    row = lax.broadcasted_iota(jnp.int32, (length, length), 0)
    col = lax.broadcasted_iota(jnp.int32, (length, length), 1)
    expert_r = lax.broadcasted_iota(jnp.int32, (max(n_sp, 16), length), 0)
    in_r = ((routes_r[0:1, :] == expert_r) | (routes_r[1:2, :] == expert_r)).astype(F32)
    rank_r = jnp.dot(in_r.astype(BF16), (row < col).astype(F32).astype(BF16), preferred_element_type=F32)
    expert_c = lax.broadcasted_iota(jnp.int32, (length, 128), 1).astype(F32)
    in_c = ((chosen[0] == expert_c) | (chosen[1] == expert_c)).astype(F32)
    rank_c = jnp.dot((row > col).astype(F32).astype(BF16), in_c.astype(BF16), preferred_element_type=F32)
    rank_r = jnp.where(in_r > 0, rank_r, -1.0)
    rank_c = jnp.where(in_c > 0, rank_c, -1.0)

    for r in range(n_tp - 1, 0, -1):
        arrived(mixb.at[r, piece_rows(0)], mx_r.at[0, r])
        if len(masks) == 2:
            pass_on(r, 0, 1)
        if masks:
            pass_on(r, 0, 2)
    loads[3].wait()
    loads[4].wait()
    total = own[...].astype(F32) + jnp.dot(gbuf[0], mixb[0], preferred_element_type=F32)
    if len(masks) == 2:
        for r in range(n_tp - 1, 0, -1):
            arrived(mixb.at[r, piece_rows(2)], mx_r.at[1, r])
            pass_on(r, 2, 3)
    for r in range(n_tp - 1, 0, -1):
        if masks:
            arrived(mixb.at[r, piece_rows(1)], mx_r.at[2, r])
        if len(masks) == 2:
            arrived(mixb.at[r, piece_rows(3)], mx_r.at[3, r])
        arrived(gbuf.at[r], ga_r.at[r])
        total = total + jnp.dot(gbuf[r], mixb[r], preferred_element_type=F32)
    hidden[...] = total
    scaled = (total * gain[:, pl.ds(at(p), width)]).astype(BF16)

    slot_r = lax.broadcasted_iota(jnp.int32, (cap, length), 0).astype(F32)
    turn = [0, 1, 2, 3, 4, 6, 5, 7] + list(range(8, n_sp))
    for d in range(n_sp):
        e = xor(s, turn[d], n_sp)
        line = jnp.sum(jnp.where(expert_r == e, rank_r, 0.0), axis=0, keepdims=True)
        pick = (line == slot_r).astype(F32).astype(BF16)
        rows = jnp.dot(pick, scaled, preferred_element_type=F32).astype(BF16)
        if d == 0:
            xbuf[0, 0] = rows
        else:
            obuf[d] = rows
            send(obuf.at[d], xbuf.at[0, d], z_s.at[d], z_r.at[d], sp=e)

    def axes(d):
        side = lax.rem(s + d, 2) * (x_side - 1) if square else 0
        return 1 + side, x_side - side

    def gather_first(d):
        u, _ = axes(d)
        if d:
            arrived(xbuf.at[0, d], z_r.at[d])
        for k in firsts[1:]:
            f = k * u
            send(xbuf.at[0, d], xbuf.at[f, d], ag_s.at[d, f], ag_r.at[d, f], tp=xor(p, f, n_tp))

    def gather_second(d):
        u, v = axes(d)
        for k in firsts:
            f = k * u
            if k:
                arrived(xbuf.at[f, d], ag_r.at[d, f])
            for l in seconds[1:]:
                g = l * v
                send(
                    xbuf.at[f, d], xbuf.at[f + g, d], ag_s.at[d, f + g], ag_r.at[d, f + g],
                    tp=xor(p, g, n_tp),
                )

    tile = min(256, hidden_units)
    tiles = hidden_units // tile

    scales = {}

    def up_part(d, low, high):
        def up_tile(j, _):
            lanes = pl.ds(pl.multiple_of(j * tile, tile), tile)
            gate = jnp.zeros((cap, tile), F32)
            upper = jnp.zeros((cap, tile), F32)
            for r in range(n_tp):
                lhs = xbuf[r, d]
                deep = pl.ds(at(xor(p, r, n_tp)), width)
                gate = gate + jnp.dot(lhs, wg[deep, lanes], preferred_element_type=F32)
                upper = upper + jnp.dot(lhs, wu[deep, lanes], preferred_element_type=F32)
            gate, upper = gate * scales[d], upper * scales[d]
            act[:, lanes] = (gate / (1.0 + jnp.exp(-gate)) * upper).astype(BF16)
            return 0

        lax.fori_loop(low, high, up_tile, 0)

    def up_first(d):
        u, v = axes(d)
        for k in firsts:
            for l in seconds[1:]:
                arrived(xbuf.at[k * u + l * v, d], ag_r.at[d, k * u + l * v])
        power = jnp.zeros((cap, 1), F32)
        for r in range(n_tp):
            inverse = 1.0 / gain[:, pl.ds(at(xor(p, r, n_tp)), width)]
            plain = xbuf[r, d].astype(F32) * inverse
            power = power + jnp.sum(plain * plain, axis=1, keepdims=True)
        scales[d] = lax.rsqrt(power / features + 1e-06)
        up_part(d, 0, tiles // 2)

    def up_second(d):
        up_part(d, tiles // 2, tiles)

    def down_part(d, low, high):
        u, v = axes(d)
        for k in range(low, high):
            for l in seconds[::-1]:
                r = k * u + l * v
                lanes = pl.ds(at(xor(p, r, n_tp)), width)
                pbuf[r, d] = jnp.dot(act[...], wd[:, lanes], preferred_element_type=F32).astype(BF16)

    def down_first(d):
        down_part(d, 1, len(firsts))

    def down_second(d):
        down_part(d, 0, 1)

    def scatter_first(d):
        u, v = axes(d)
        for k in firsts[:0:-1]:
            for l in seconds[::-1]:
                r = k * u + l * v
                send(pbuf.at[r, d], r1.at[r, d], rs_s.at[d, r], rs_r.at[d, r], tp=xor(p, k * u, n_tp))

    def scatter_second(d):
        u, v = axes(d)
        for l in seconds[1:]:
            g = l * v
            part = pbuf[g, d].astype(F32)
            for k in firsts[1:]:
                arrived(r1.at[k * u + g, d], rs_r.at[d, k * u + g])
                part = part + r1[k * u + g, d].astype(F32)
            pbuf[g, d] = part.astype(BF16)
            send(pbuf.at[g, d], r1.at[g, d], rs_s.at[d, g], rs_r.at[d, g], tp=xor(p, g, n_tp))

    def give_back(d):
        u, v = axes(d)
        part = pbuf[0, d].astype(F32)
        for k in [k * u for k in firsts[1:]] + [l * v for l in seconds[1:]]:
            arrived(r1.at[k, d], rs_r.at[d, k])
            part = part + r1[k, d].astype(F32)
        if d == 0:
            back[0] = part.astype(BF16)
        else:
            ret[d] = part.astype(BF16)
            send(ret.at[d], back.at[d], bk_s.at[d], bk_r.at[d], sp=xor(s, turn[d], n_sp))

    slot_c = lax.broadcasted_iota(jnp.int32, (length, cap), 1).astype(F32)
    acc[...] = hidden[...]

    def combine(d):
        e = xor(s, turn[d], n_sp)
        if d:
            arrived(back.at[d], bk_r.at[d])
        line = jnp.sum(jnp.where(expert_c == e.astype(F32), rank_c, 0.0), axis=1, keepdims=True)
        pick = (line == slot_c).astype(F32).astype(BF16)
        fetched = jnp.dot(pick, back[d], preferred_element_type=F32)
        weight = sum(jnp.where(c == e.astype(F32), w, 0.0) for c, w in zip(chosen, chosen_weight))
        acc[...] = acc[...] + fetched * weight

    stages = (
        gather_first, gather_second, up_first, up_second, down_first,
        scatter_first, down_second, scatter_second, give_back, combine,
    )
    plan = TUNED if len(TUNED) == len(stages) * n_sp else general_plan(n_sp)
    weights_here = False
    for k, d in plan:
        stage = stages[k]
        if stage is up_first and not weights_here:
            weights_here = True
            for load in weight_loads:
                load.wait()
        stage(d)
    out[...] = acc[...].astype(out.dtype)
    for copy in sends:
        copy.wait_send()

    @pl.when(has_next)
    def _():
        rim.wait_send()


def body(
    outer_gate, inner_gate, values, conv_taps, document, mix_proj, stream, norm_gain,
    routes, route_weight, w_gate, w_up, w_down,
):
    length, features = stream.shape
    channels = outer_gate.shape[1]
    n_sp, n_tp = lax.axis_size("sp"), lax.axis_size("tp")
    width = features // n_tp
    units = w_gate.shape[2]
    cap = -(-(3 * length // n_sp) // 16) * 16
    vmem, hbm = pl.BlockSpec(memory_space=pltpu.VMEM), pl.BlockSpec(memory_space=pltpu.HBM)
    block = (n_sp, cap, width)
    dma = pltpu.SemaphoreType.DMA
    return pl.pallas_call(
        functools.partial(kernel, n_sp, n_tp, cap),
        out_shape=pltpu.VMEM((length, width), BF16),
        in_specs=[hbm] * 13,
        out_specs=vmem,
        scratch_shapes=[
            pltpu.VMEM(conv_taps.shape, BF16),
            pltpu.VMEM((1, length), jnp.int32),
            pltpu.VMEM((2, length), jnp.int32),
            pltpu.VMEM((2, length), F32),
            pltpu.VMEM((1, features), F32),
            pltpu.VMEM((length, channels), BF16),
            pltpu.VMEM((length, channels), BF16),
            pltpu.VMEM((length, channels), BF16),
            pltpu.VMEM((length, width), BF16),
            pltpu.VMEM((features, units), BF16),
            pltpu.VMEM((features, units), BF16),
            pltpu.VMEM((units, features), BF16),
            pltpu.VMEM((16, channels), F32),
            pltpu.VMEM((16, channels), F32),
            pltpu.VMEM((length + 8, channels), F32),
            pltpu.VMEM((length + 8, channels), F32),
            pltpu.VMEM((n_tp, length, channels), BF16),
            pltpu.VMEM((n_tp, channels, width), BF16),
            pltpu.VMEM((length, width), F32),
            pltpu.VMEM(block, BF16),
            pltpu.VMEM((n_tp,) + block, BF16),
            pltpu.VMEM((n_tp,) + block, BF16),
            pltpu.VMEM((n_tp,) + block, BF16),
            pltpu.VMEM((cap, units), BF16),
            pltpu.VMEM(block, BF16),
            pltpu.VMEM(block, BF16),
            pltpu.VMEM((length, width), F32),
            dma((13,)), dma, dma, dma((n_tp,)), dma((n_tp,)), dma((4, n_tp)), dma((4, n_tp)), dma((n_sp,)), dma((n_sp,)),
            dma((n_sp, n_tp)), dma((n_sp, n_tp)), dma((n_sp, n_tp)), dma((n_sp, n_tp)),
            dma((n_sp,)), dma((n_sp,)),
        ],
        compiler_params=pltpu.CompilerParams(
            collective_id=0, has_side_effects=True, vmem_limit_bytes=40 << 20
        ),
    )(*[pltpu.with_memory_space_constraint(x, pltpu.HBM) for x in (
        conv_taps, document.reshape(1, -1), routes.T, route_weight.T, norm_gain.reshape(1, -1),
        outer_gate, inner_gate, values, mix_proj, stream, w_gate, w_up, w_down,
    )])


def solution(mesh):
    return jax.shard_map(
        body,
        mesh=mesh,
        in_specs=(
            P("sp", "tp"),
            P("sp", "tp"),
            P("sp", "tp"),
            P(None, "tp"),
            P("sp"),
            P("tp", None),
            P("sp", None),
            P(),
            P("sp", None),
            P("sp", None),
            P("sp", None, "tp"),
            P("sp", None, "tp"),
            P("sp", "tp", None),
        ),
        out_specs=P("sp", "tp"),
        check_vma=False,
    )
```

time: 88.6 us -> 79.7 us (0.90)
  Pallas kernels: 86.7 us -> 78.3 us
  local copies, waits for them, and re-layouts: 1.67 us -> 0.71 us
    pallas_call x1, Pallas kernels: 86.7 us -> 78.3 us  [body(): pl.pallas_call(functools.partial(kernel, n_sp, n_tp, cap), out_shape=pltp...]
    unnamed x1, local copies, waits for them, and re-layouts: 1.67 us -> 0.71 us
where the time goes in v1:
time: 79.7 us; the launch traced here: 79.1 us
  Pallas kernels  78.3 us (98%)
    pallas_call x1, Pallas kernels, body(): pl.pallas_call(functools.partial(kernel, n_sp, n_tp, cap), out_shape=pltp...  78.3 us

profile of v1, /device:TPU:1, one launch (start us, length us, event | category | flops | bytes accessed | tf_op | source)
XLA Modules:
  0.0 79.1 jit_solution(10073370179330227933)
XLA Ops:
  0.0 78.3 %shard_map.127 = bf16[256,512]{1,0:T(8,128)(2,1)S(1)} custom-call(bf16[3,256]{1,0:T(4,128)(2,1)} %taps_hbm.1, s32[1,256]{1,0:T(1,128)} %bitcast.7, s32[2,256]{1,0:T(2,128)} %bitcast.5, f32[2,256]{1,0:T(2,128)} %bitcast.6, f32[1,2048]{1,0:T(1,128)} %bitcast.4, bf16[256,256]{1,0:T(8,128)(2,1)} %outer_hbm.1, bf16[256,256]{1,0:T(8,128)(2,1)} %inner_hbm.1, ...), custom_call_target="tpu_custom_call" | custom-call | tf_op jit(solution)/shard_map/pallas_call | solution.py:413
  78.3 0.7 copy.15

commit v2 on v1

--- a/solution.py
+++ b/solution.py
@@ -12,41 +12,51 @@
 MESH = pl.DeviceIdType.MESH
 HEAD = 16
 TUNED = (
-    (0, 1), (0, 0), (1, 0), (1, 1), (0, 2), (0, 3), (0, 4), (1, 2), (2, 1), (1, 3),
-    (0, 5), (1, 4), (3, 1), (4, 1), (6, 1), (0, 6), (1, 5), (2, 2), (0, 7), (3, 2),
-    (4, 2), (6, 2), (1, 6), (2, 3), (5, 2), (3, 3), (4, 3), (5, 3), (1, 7), (6, 3),
-    (2, 4), (3, 4), (4, 4), (6, 4), (2, 6), (7, 2), (5, 4), (3, 6), (7, 3), (4, 6),
-    (6, 6), (5, 6), (2, 5), (8, 2), (3, 5), (4, 5), (7, 4), (5, 5), (6, 5), (8, 3),
-    (2, 7), (3, 7), (7, 6), (4, 7), (8, 4), (5, 7), (6, 7), (2, 0), (9, 3), (7, 5),
-    (8, 6), (9, 2), (5, 1), (3, 0), (4, 0), (6, 0), (7, 7), (8, 5), (5, 0), (8, 7),
-    (7, 1), (9, 4), (7, 0), (9, 6), (9, 5), (8, 1), (9, 1), (9, 7), (8, 0), (9, 0),
+    (0, 0), (1, 0), (0, 1), (0, 2), (1, 1), (0, 4), (1, 2), (0, 3),
+    (0, 5), (1, 4), (2, 0), (0, 6), (1, 5), (0, 7), (3, 0), (4, 0),
+    (6, 0), (1, 6), (1, 3), (2, 2), (1, 7), (3, 2), (4, 2), (5, 5),
+    (6, 2), (5, 4), (5, 0), (2, 3), (7, 5), (3, 3), (4, 3), (6, 3),
+    (5, 6), (7, 4), (2, 1), (5, 7), (8, 5), (3, 1), (4, 1), (7, 6),
+    (5, 3), (8, 4), (5, 2), (9, 5), (8, 6), (7, 7), (6, 1), (7, 3),
+    (5, 1), (9, 4), (8, 7), (7, 2), (8, 3), (7, 1), (7, 0), (8, 2),
+    (9, 3), (8, 1), (9, 6), (8, 0), (9, 0), (9, 7), (9, 1), (9, 2),
 )
 
 
-def general_plan(n_sp):
+def general_plan(n_sp, group):
     plan, near = [], min(2, n_sp)
 
     def run(k, d, low=0):
         if low <= d < n_sp and (k, d) not in plan:
             plan.append((k, d))
 
-    for k, d in ((0, 0), (0, 1), (1, 0), (0, 2), (1, 1), (0, 3)):
+    for k, d in ((0, 0), (0, 1), (1, 0), (1, 1), (0, 2), (0, 3), (1, 2)):
         run(k, d)
-    for d in range(n_sp):
-        run(2, d)
-        run(1, d + 2)
-        run(3, d)
-        run(0, d + 4)
-        run(4, d)
-        run(5, d, near)
-        run(6, d)
-        run(7, d - 2, near)
-        run(8, d - 4, near)
-        run(9, d - 7, near)
-    for d in (n_sp - 2, n_sp - 1):
-        run(8, d - 2, near)
+    for j in range(n_sp // group):
+        first = j * group
+        ahead, behind = range(first + 3, first + 3 + group), range(first - group, first)
+        plan.append((2, j))
+        for d in ahead:
+            run(0, d + 1)
+        plan.append((3, j))
+        for d in ahead:
+            run(1, d)
+        plan.append((4, j))
+        for d in range(first, first + group):
+            run(5, d, near)
+        plan.append((6, j))
+        for d in behind:
+            run(7, d, near)
+        for d in behind:
+            run(8, d - group, near)
+        for d in behind:
+            run(9, d - 3 * group, near)
+    for d in range(near, n_sp):
+        run(8, d - group, near)
         run(7, d, near)
         run(5, n_sp - 1 - d)
+    for d in (1, 0):
+        run(5, d)
     for d in range(near, n_sp):
         run(8, d)
     for d in (1, 0):
@@ -91,10 +101,18 @@
     while x_side * x_side < n_tp:
         x_side *= 2
     square = x_side * x_side == n_tp
+    group = 2 if n_sp % 2 == 0 else 1
     firsts, seconds = range(x_side), range(n_tp // x_side)
 
     def at(index):
         return pl.multiple_of(index * width, width)
+
+    masks = [m for m in (2, 1) if m < n_sp]
+    pieces = 2 ** len(masks)
+    piece = channels // pieces
+
+    def piece_rows(mask):
+        return pl.ds(pl.multiple_of(lax.rem(xor(s, mask, n_sp), pieces) * piece, piece), piece)
 
     loads = [
         pltpu.make_async_copy(inner_hbm, inner, local_sem.at[0]),
@@ -122,39 +140,27 @@
         pl.semaphore_signal(barrier, inc=1, device_id={"sp": xor(s, d, n_sp)}, device_id_type=MESH)
     for r in range(1, n_tp):
         pl.semaphore_signal(barrier, inc=1, device_id={"tp": xor(p, r, n_tp)}, device_id_type=MESH)
-    sends = []
-
     def send(src, dst, s_sem, r_sem, **device):
-        copy = pltpu.make_async_remote_copy(
+        pltpu.make_async_remote_copy(
             src_ref=src, dst_ref=dst, send_sem=s_sem, recv_sem=r_sem,
             device_id=device, device_id_type=MESH,
-        )
-        copy.start()
-        sends.append(copy)
-        return copy
+        ).start()
 
     def arrived(ref, sem):
         pltpu.make_async_copy(ref, ref, sem).wait()
-
-    masks = [m for m in (2, 1) if m < n_sp]
-    pieces = 2 ** len(masks)
-    piece = channels // pieces
-
-    def piece_rows(mask):
-        return pl.ds(pl.multiple_of(lax.rem(xor(s, mask, n_sp), pieces) * piece, piece), piece)
 
     pl.semaphore_wait(barrier, n_sp - 1 + n_tp - 1)
     for r in range(n_tp - 1, 0, -1):
         peer = xor(p, r, n_tp)
         send(
             mix_hbm.at[piece_rows(0), pl.ds(at(peer), width)], mixb.at[r, piece_rows(0)],
-            mx_s.at[0, r], mx_r.at[0, r], tp=peer,
+            mx_s, mx_r.at[0, r], tp=peer,
         )
 
     def pass_on(r, mask, step):
         send(
             mixb.at[r, piece_rows(mask)], mixb.at[r, piece_rows(mask)],
-            mx_s.at[step, r], mx_r.at[step, r], sp=xor(s, masks[-1] if step != 1 else masks[0], n_sp),
+            mx_s, mx_r.at[step, r], sp=xor(s, masks[-1] if step != 1 else masks[0], n_sp),
         )
 
     for load in small_loads:
@@ -205,7 +211,7 @@
         gbuf[0, :HEAD] = gated(HEAD)
 
     for r in range(n_tp - 1, 0, -1):
-        send(gbuf.at[0], gbuf.at[r], ga_s.at[r], ga_r.at[r], tp=xor(p, r, n_tp))
+        send(gbuf.at[0], gbuf.at[r], ga_s, ga_r.at[r], tp=xor(p, r, n_tp))
     for load in weight_loads:
         load.start()
 
@@ -219,6 +225,13 @@
     rank_c = jnp.dot((row > col).astype(F32).astype(BF16), in_c.astype(BF16), preferred_element_type=F32)
     rank_r = jnp.where(in_r > 0, rank_r, -1.0)
     rank_c = jnp.where(in_c > 0, rank_c, -1.0)
+
+    slot_r = lax.broadcasted_iota(jnp.int32, (cap, length), 0).astype(F32)
+    turn = [0, 1, 2, 3, 4, 6, 5, 7] + list(range(8, n_sp))
+    picks = []
+    for d in range(n_sp):
+        line = jnp.sum(jnp.where(expert_r == xor(s, turn[d], n_sp), rank_r, 0.0), axis=0, keepdims=True)
+        picks.append((line == slot_r).astype(F32).astype(BF16))
 
     for r in range(n_tp - 1, 0, -1):
         arrived(mixb.at[r, piece_rows(0)], mx_r.at[0, r])
@@ -243,21 +256,16 @@
     hidden[...] = total
     scaled = (total * gain[:, pl.ds(at(p), width)]).astype(BF16)
 
-    slot_r = lax.broadcasted_iota(jnp.int32, (cap, length), 0).astype(F32)
-    turn = [0, 1, 2, 3, 4, 6, 5, 7] + list(range(8, n_sp))
     for d in range(n_sp):
-        e = xor(s, turn[d], n_sp)
-        line = jnp.sum(jnp.where(expert_r == e, rank_r, 0.0), axis=0, keepdims=True)
-        pick = (line == slot_r).astype(F32).astype(BF16)
-        rows = jnp.dot(pick, scaled, preferred_element_type=F32).astype(BF16)
+        rows = jnp.dot(picks[d], scaled, preferred_element_type=F32).astype(BF16)
         if d == 0:
             xbuf[0, 0] = rows
         else:
             obuf[d] = rows
-            send(obuf.at[d], xbuf.at[0, d], z_s.at[d], z_r.at[d], sp=e)
+            send(obuf.at[d], xbuf.at[0, d], z_s, z_r.at[d], sp=xor(s, turn[d], n_sp))
 
     def axes(d):
-        side = lax.rem(s + d, 2) * (x_side - 1) if square else 0
+        side = lax.rem(s + d // group, 2) * (x_side - 1) if square else 0
         return 1 + side, x_side - side
 
     def gather_first(d):
@@ -266,7 +274,7 @@
             arrived(xbuf.at[0, d], z_r.at[d])
         for k in firsts[1:]:
             f = k * u
-            send(xbuf.at[0, d], xbuf.at[f, d], ag_s.at[d, f], ag_r.at[d, f], tp=xor(p, f, n_tp))
+            send(xbuf.at[0, d], xbuf.at[f, d], ag_s, ag_r.at[d, f], tp=xor(p, f, n_tp))
 
     def gather_second(d):
         u, v = axes(d)
@@ -277,7 +285,7 @@
             for l in seconds[1:]:
                 g = l * v
                 send(
-                    xbuf.at[f, d], xbuf.at[f + g, d], ag_s.at[d, f + g], ag_r.at[d, f + g],
+                    xbuf.at[f, d], xbuf.at[f + g, d], ag_s, ag_r.at[d, f + g],
                     tp=xor(p, g, n_tp),
                 )
 
@@ -286,58 +294,66 @@
 
     scales = {}
 
-    def up_part(d, low, high):
-        def up_tile(j, _):
-            lanes = pl.ds(pl.multiple_of(j * tile, tile), tile)
-            gate = jnp.zeros((cap, tile), F32)
-            upper = jnp.zeros((cap, tile), F32)
+    def members(j):
+        return slice(j * group, (j + 1) * group)
+
+    def up_part(j, low, high):
+        def up_tile(i, _):
+            lanes = pl.ds(pl.multiple_of(i * tile, tile), tile)
+            gate = jnp.zeros((group * cap, tile), F32)
+            upper = jnp.zeros((group * cap, tile), F32)
             for r in range(n_tp):
-                lhs = xbuf[r, d]
+                lhs = xbuf[r, members(j)].reshape(group * cap, width)
                 deep = pl.ds(at(xor(p, r, n_tp)), width)
                 gate = gate + jnp.dot(lhs, wg[deep, lanes], preferred_element_type=F32)
                 upper = upper + jnp.dot(lhs, wu[deep, lanes], preferred_element_type=F32)
-            gate, upper = gate * scales[d], upper * scales[d]
+            gate, upper = gate * scales[j], upper * scales[j]
             act[:, lanes] = (gate / (1.0 + jnp.exp(-gate)) * upper).astype(BF16)
             return 0
 
         lax.fori_loop(low, high, up_tile, 0)
 
-    def up_first(d):
-        u, v = axes(d)
-        for k in firsts:
-            for l in seconds[1:]:
-                arrived(xbuf.at[k * u + l * v, d], ag_r.at[d, k * u + l * v])
-        power = jnp.zeros((cap, 1), F32)
+    def up_first(j):
+        if not scales:
+            for load in weight_loads:
+                load.wait()
+        u, v = axes(j * group)
+        for d in range(j * group, (j + 1) * group):
+            for k in firsts:
+                for l in seconds[1:]:
+                    arrived(xbuf.at[k * u + l * v, d], ag_r.at[d, k * u + l * v])
+        power = jnp.zeros((group * cap, 1), F32)
         for r in range(n_tp):
             inverse = 1.0 / gain[:, pl.ds(at(xor(p, r, n_tp)), width)]
-            plain = xbuf[r, d].astype(F32) * inverse
+            plain = xbuf[r, members(j)].reshape(group * cap, width).astype(F32) * inverse
             power = power + jnp.sum(plain * plain, axis=1, keepdims=True)
-        scales[d] = lax.rsqrt(power / features + 1e-06)
-        up_part(d, 0, tiles // 2)
-
-    def up_second(d):
-        up_part(d, tiles // 2, tiles)
-
-    def down_part(d, low, high):
-        u, v = axes(d)
+        scales[j] = lax.rsqrt(power / features + 1e-06)
+        up_part(j, 0, tiles // 2)
+
+    def up_second(j):
+        up_part(j, tiles // 2, tiles)
+
+    def down_part(j, low, high):
+        u, v = axes(j * group)
         for k in range(low, high):
             for l in seconds[::-1]:
                 r = k * u + l * v
                 lanes = pl.ds(at(xor(p, r, n_tp)), width)
-                pbuf[r, d] = jnp.dot(act[...], wd[:, lanes], preferred_element_type=F32).astype(BF16)
-
-    def down_first(d):
-        down_part(d, 1, len(firsts))
-
-    def down_second(d):
-        down_part(d, 0, 1)
+                part = jnp.dot(act[...], wd[:, lanes], preferred_element_type=F32).astype(BF16)
+                pbuf[r, members(j)] = part.reshape(group, cap, width)
+
+    def down_first(j):
+        down_part(j, 1, len(firsts))
+
+    def down_second(j):
+        down_part(j, 0, 1)
 
     def scatter_first(d):
         u, v = axes(d)
         for k in firsts[:0:-1]:
             for l in seconds[::-1]:
                 r = k * u + l * v
-                send(pbuf.at[r, d], r1.at[r, d], rs_s.at[d, r], rs_r.at[d, r], tp=xor(p, k * u, n_tp))
+                send(pbuf.at[r, d], r1.at[r, d], rs_s, rs_r.at[d, r], tp=xor(p, k * u, n_tp))
 
     def scatter_second(d):
         u, v = axes(d)
@@ -348,7 +364,7 @@
                 arrived(r1.at[k * u + g, d], rs_r.at[d, k * u + g])
                 part = part + r1[k * u + g, d].astype(F32)
             pbuf[g, d] = part.astype(BF16)
-            send(pbuf.at[g, d], r1.at[g, d], rs_s.at[d, g], rs_r.at[d, g], tp=xor(p, g, n_tp))
+            send(pbuf.at[g, d], r1.at[g, d], rs_s, rs_r.at[d, g], tp=xor(p, g, n_tp))
 
     def give_back(d):
         u, v = axes(d)
@@ -360,7 +376,7 @@
             back[0] = part.astype(BF16)
         else:
             ret[d] = part.astype(BF16)
-            send(ret.at[d], back.at[d], bk_s.at[d], bk_r.at[d], sp=xor(s, turn[d], n_sp))
+            send(ret.at[d], back.at[d], bk_s, bk_r.at[d], sp=xor(s, turn[d], n_sp))
 
     slot_c = lax.broadcasted_iota(jnp.int32, (length, cap), 1).astype(F32)
     acc[...] = hidden[...]
@@ -379,19 +395,18 @@
         gather_first, gather_second, up_first, up_second, down_first,
         scatter_first, down_second, scatter_second, give_back, combine,
     )
-    plan = TUNED if len(TUNED) == len(stages) * n_sp else general_plan(n_sp)
-    weights_here = False
-    for k, d in plan:
-        stage = stages[k]
-        if stage is up_first and not weights_here:
-            weights_here = True
-            for load in weight_loads:
-                load.wait()
-        stage(d)
+    plan = general_plan(n_sp, group)
+    plan = TUNED if len(TUNED) == len(plan) else plan
+    for k, d in plan[:-1]:
+        stages[k](d)
+    arrived(xbuf.at[0, pl.ds(1, n_sp - 1)], z_s)
+    arrived(back.at[pl.ds(1, n_sp - 1)], bk_s)
+    arrived(gbuf.at[pl.ds(1, n_tp - 1)], ga_s)
+    arrived(xbuf.at[pl.ds(1, n_tp - 1)], ag_s)
+    arrived(r1.at[pl.ds(1, n_tp - 1)], rs_s)
+    arrived(mixb.at[pl.ds(1, n_tp - 1)], mx_s)
+    stages[plan[-1][0]](plan[-1][1])
     out[...] = acc[...].astype(out.dtype)
-    for copy in sends:
-        copy.wait_send()
-
     @pl.when(has_next)
     def _():
         rim.wait_send()
@@ -439,13 +454,13 @@
             pltpu.VMEM((n_tp,) + block, BF16),
             pltpu.VMEM((n_tp,) + block, BF16),
             pltpu.VMEM((n_tp,) + block, BF16),
-            pltpu.VMEM((cap, units), BF16),
+            pltpu.VMEM(((2 if n_sp % 2 == 0 else 1) * cap, units), BF16),
             pltpu.VMEM(block, BF16),
             pltpu.VMEM(block, BF16),
             pltpu.VMEM((length, width), F32),
-            dma((13,)), dma, dma, dma((n_tp,)), dma((n_tp,)), dma((4, n_tp)), dma((4, n_tp)), dma((n_sp,)), dma((n_sp,)),
-            dma((n_sp, n_tp)), dma((n_sp, n_tp)), dma((n_sp, n_tp)), dma((n_sp, n_tp)),
-            dma((n_sp,)), dma((n_sp,)),
+            dma((13,)), dma, dma, dma, dma((n_tp,)), dma, dma((4, n_tp)), dma, dma((n_sp,)),
+            dma, dma((n_sp, n_tp)), dma, dma((n_sp, n_tp)),
+            dma, dma((n_sp,)),
         ],
         compiler_params=pltpu.CompilerParams(
             collective_id=0, has_side_effects=True, vmem_limit_bytes=40 << 20

time: 79.7 us -> 78.9 us (0.990)
  no operation moved by 1% of the time
where the time goes in v2:
time: 78.9 us; the launch traced here: 78.3 us
  Pallas kernels  77.6 us (98%)
    pallas_call x1, Pallas kernels, body(): pl.pallas_call(functools.partial(kernel, n_sp, n_tp, cap), out_shape=pltp...  77.6 us

profile of v2, /device:TPU:1, one launch (start us, length us, event | category | flops | bytes accessed | tf_op | source)
XLA Modules:
  0.0 78.3 jit_solution(10069417819631122174)
XLA Ops:
  0.0 77.6 %shard_map.127 = bf16[256,512]{1,0:T(8,128)(2,1)S(1)} custom-call(bf16[3,256]{1,0:T(4,128)(2,1)} %taps_hbm.1, s32[1,256]{1,0:T(1,128)} %bitcast.7, s32[2,256]{1,0:T(2,128)} %bitcast.5, f32[2,256]{1,0:T(2,128)} %bitcast.6, f32[1,2048]{1,0:T(1,128)} %bitcast.4, bf16[256,256]{1,0:T(8,128)(2,1)} %outer_hbm.1, bf16[256,256]{1,0:T(8,128)(2,1)} %inner_hbm.1, ...), custom_call_target="tpu_custom_call" | custom-call | tf_op jit(solution)/shard_map/pallas_call | solution.py:428
  77.6 0.7 copy.15

commit v3 on v2

--- a/solution.py
+++ b/solution.py
@@ -227,7 +227,7 @@
     rank_c = jnp.where(in_c > 0, rank_c, -1.0)
 
     slot_r = lax.broadcasted_iota(jnp.int32, (cap, length), 0).astype(F32)
-    turn = [0, 1, 2, 3, 4, 6, 5, 7] + list(range(8, n_sp))
+    turn = [0, 1, 3, 2, 5, 7, 4, 6] + list(range(8, n_sp))
     picks = []
     for d in range(n_sp):
         line = jnp.sum(jnp.where(expert_r == xor(s, turn[d], n_sp), rank_r, 0.0), axis=0, keepdims=True)

time: 78.9 us -> 78.4 us (level)
  no operation moved by 1% of the time
where the time goes in v3:
time: 78.4 us; the launch traced here: 78.1 us
  Pallas kernels  77.3 us (99%)
    pallas_call x1, Pallas kernels, body(): pl.pallas_call(functools.partial(kernel, n_sp, n_tp, cap), out_shape=pltp...  77.3 us

profile of v3, /device:TPU:1, one launch (start us, length us, event | category | flops | bytes accessed | tf_op | source)
XLA Modules:
  0.0 78.1 jit_solution(16819696460408446192)
XLA Ops:
  0.0 77.3 %shard_map.127 = bf16[256,512]{1,0:T(8,128)(2,1)S(1)} custom-call(bf16[3,256]{1,0:T(4,128)(2,1)} %taps_hbm.1, s32[1,256]{1,0:T(1,128)} %bitcast.7, s32[2,256]{1,0:T(2,128)} %bitcast.5, f32[2,256]{1,0:T(2,128)} %bitcast.6, f32[1,2048]{1,0:T(1,128)} %bitcast.4, bf16[256,256]{1,0:T(8,128)(2,1)} %outer_hbm.1, bf16[256,256]{1,0:T(8,128)(2,1)} %inner_hbm.1, ...), custom_call_target="tpu_custom_call" | custom-call | tf_op jit(solution)/shard_map/pallas_call | solution.py:428
  77.4 0.7 copy.15
